TPU v7x, 32 devices: a whole 2x2x4 slice. The times are simulated.
32 devices in a mesh: grp: 2 (over y), dp: 2 (over x), kv: 4 (over z), tp: 2 (over core).
Axes of the slice: x: 2, y: 2, z: 4, core: 2. Of those that a mesh axis runs over, the one named last changes fastest.
Arguments:
- residual_input: bfloat16 [128, 4096], P(('grp', 'dp', 'tp'), 'kv'), parts along dimension 0, may hold values from -6 to 6
- incoming_state: float32 [128, 16, 64, 128], P(('grp', 'kv'), ('dp', 'tp')), parts along dimension 0, may hold values from -4 to 4
- extra_log_decay: float32 [128, 1024], P(('grp', 'kv'), ('dp', 'tp')), parts along dimension 0, may hold values from -0.7 to 0
- leading_norm_gain: float32 [4096], P('kv'), may hold values from 0.1 to 1.9
- leading_gate_weight: bfloat16 [4096, 11264], P('kv', ('dp', 'tp')), may hold values from -0.09375 to 0.09375
- leading_up_weight: bfloat16 [4096, 11264], P('kv', ('dp', 'tp')), may hold values from -0.09375 to 0.09375
- leading_down_weight: bfloat16 [11264, 4096], P(('dp', 'tp'), 'kv'), may hold values from -0.0546875 to 0.0546875
- attention_norm_gain: float32 [4096], P('kv'), may hold values from 0.1 to 1.9
- query_projector: bfloat16 [4096, 1024], P('kv', ('dp', 'tp')), may hold values from -0.09375 to 0.09375
- key_projector: bfloat16 [4096, 1024], P('kv', ('dp', 'tp')), may hold values from -0.09375 to 0.09375
- value_projector: bfloat16 [4096, 2048], P('kv', ('dp', 'tp')), may hold values from -0.09375 to 0.09375
- output_gate_weight: bfloat16 [4096, 2048], P('kv', ('dp', 'tp')), may hold values from -0.09375 to 0.09375
- forget_weight: bfloat16 [4096, 1024], P('kv', ('dp', 'tp')), may hold values from -0.75 to 0.75
- head_norm_gain: float32 [128], replicated, may hold values from 0.1 to 1.9
- output_projector: bfloat16 [2048, 4096], P(('dp', 'tp'), 'kv'), may hold values from -0.125 to 0.125
- trailing_norm_gain: float32 [4096], P('kv'), may hold values from 0.1 to 1.9
- trailing_gate_weight: bfloat16 [4096, 11264], P('kv', ('dp', 'tp')), may hold values from -0.09375 to 0.09375
- trailing_up_weight: bfloat16 [4096, 11264], P('kv', ('dp', 'tp')), may hold values from -0.09375 to 0.09375
- trailing_down_weight: bfloat16 [11264, 4096], P(('dp', 'tp'), 'kv'), may hold values from -0.0546875 to 0.0546875
Outputs:
- result: bfloat16 [128, 4096], P(('grp', 'dp', 'tp'), 'kv'), parts along dimension 0
- new_state: float32 [128, 16, 64, 128], P(('grp', 'kv'), ('dp', 'tp')), parts along dimension 0
There are 2 independent parts, one for each index of `grp`. A program takes and returns all parts, laid end to end along the dimension named above; an argument that names none is the same for every part. Nothing has to cross between parts.
All inputs are finite; a program needn't handle non-finite values.
Results may differ from a plain program's by a relative error of at most 0.0095.
Values may be sent and summed in bfloat16 or wider, within the bound.
A program may use at most 128 MiB of HBM per device.

v0:
```python
import functools

import jax
import jax.numpy as jnp
from jax import lax
from jax.experimental import pallas as pl
from jax.experimental.pallas import tpu as pltpu
from jax.sharding import PartitionSpec as P

KEY_CHANNELS = 64
VALUE_DIM = 128
LANES = 128
epsilon = 1e-06
MESH = pl.DeviceIdType.MESH
F32 = jnp.float32
BF16 = jnp.bfloat16
CHUNKS = 4


def spans(width, count):
    if width % LANES:
        return [(0, width)]
    tile = 2 * LANES if width % (2 * LANES) == 0 else LANES
    tiles = width // tile
    count = min(count, tiles)
    cuts = [tile * ((tiles * i + count - 1) // count) for i in range(count + 1)]
    return list(zip(cuts[:-1], cuts[1:]))


def padded(width):
    return -(-width // LANES) * LANES


def silu(x):
    return x * jax.nn.sigmoid(x)


def kernel(dims, names, *refs):
    R, K, TP, D, B, d, F, W, V, heads = dims
    mr, mk = B // R, B // K
    ref = dict(zip(names, refs))
    dp_i, tp_i, k = lax.axis_index("dp"), lax.axis_index("tp"), lax.axis_index("kv")
    r = dp_i * TP + tp_i
    Wp = padded(W)
    kv_order = sorted(range(1, K), key=lambda o: abs(2 * o - K))
    counter = {"send": 0, "local": 0}
    pending = []

    def row_peer(o):
        t = lax.rem(r + o, R)
        return t, {"dp": t // TP, "tp": lax.rem(t, TP)}

    def kv_peer(o):
        t = lax.rem(k + o, K)
        return t, {"kv": t}

    def local(src, dst):
        i = counter["local"]
        counter["local"] += 1
        copy = pltpu.make_async_copy(src, dst, ref["local_sem"].at[i])
        copy.start()
        return copy

    def remote(src, dst, device):
        i = counter["send"]
        counter["send"] += 1
        copy = pltpu.make_async_remote_copy(
            src_ref=src,
            dst_ref=dst,
            send_sem=ref["send_sem"].at[i],
            recv_sem=ref["recv_sem"].at[i],
            device_id=device,
            device_id_type=MESH,
        )
        copy.start()
        pending.append(copy)
        return copy

    own_x = local(ref["x"], ref["x_all"].at[r])
    load_g1 = local(ref["g1"], ref["g1_v"])
    fspans = spans(F, CHUNKS)

    def load_mixer(p):
        first = []
        for a, b in fspans:
            cut = (slice(None), slice(None)) if b - a == F else (slice(None), pl.ds(a, b - a))
            first.append(
                (
                    local(ref[p + "g"].at[cut], ref[p + "g_v"].at[cut]),
                    local(ref[p + "u"].at[cut], ref[p + "u_v"].at[cut]),
                )
            )
        return first, local(ref[p + "d"], ref[p + "d_v"])

    lead = load_mixer("l")
    load_attn = [local(ref[n], ref[n + "_v"]) for n in ("g2", "wq", "wk", "wf", "wv", "wg")]
    load_state = [local(ref[n], ref[n + "_v"]) for n in ("st", "eld", "hng")]
    load_out = local(ref["wo"], ref["wo_v"])
    load_g3 = local(ref["g3"], ref["g3_v"])
    trail = load_mixer("t")

    barrier = pltpu.get_barrier_semaphore()
    for o in range(1, R):
        pl.semaphore_signal(barrier, inc=1, device_id=row_peer(o)[1], device_id_type=MESH)
    for o in kv_order:
        pl.semaphore_signal(barrier, inc=1, device_id=kv_peer(o)[1], device_id_type=MESH)
    pl.semaphore_wait(barrier, R - 1 + K - 1)

    def gather_rows(src, buf):
        copies = [remote(src, buf.at[r], row_peer(o)[1]) for o in range(1, R)]
        return copies

    def wait_all(copies):
        for copy in copies:
            copy.wait_recv()

    def normalised(buf, gain):
        wide = buf[...].reshape(B, d).astype(F32)
        squares = jnp.sum(wide * wide, axis=1, keepdims=True)
        ref["scaled"][...] = (wide * gain[...]).astype(BF16)
        return jnp.broadcast_to(squares, (B, LANES)).reshape(K, mk, LANES)

    def row_scale(total):
        return lax.rsqrt(total / D + epsilon)[:, :1]

    def mixer(p, buf, gain, loads):
        gu_loads, down_load = loads
        gu_send, gu_recv = ref[p + "gu_send"], ref[p + "gu_recv"]
        ss_send, ss_recv = ref[p + "ss_send"], ref[p + "ss_recv"]
        h_all = ref[p + "h_all"]
        ss_send[...] = normalised(buf, gain)
        ss_copies = []
        for o in kv_order:
            t, device = kv_peer(o)
            ss_copies.append(remote(ss_send.at[t], ss_recv.at[o - 1], device))
        gu_copies = []
        for (a, b), pair in zip(fspans, gu_loads):
            for i, part in enumerate("gu"):
                pair[i].wait()
                product = jnp.dot(
                    ref["scaled"][...], ref[p + part + "_v"][:, a:b], preferred_element_type=F32
                )
                gu_send[:, i, :, a:b] = product.astype(BF16).reshape(K, mk, b - a)
            group = []
            for o in kv_order:
                t, device = kv_peer(o)
                if b - a == F:
                    src, dst = gu_send.at[t], gu_recv.at[o - 1]
                else:
                    src = gu_send.at[t, :, :, pl.ds(a, b - a)]
                    dst = gu_recv.at[o - 1, :, :, pl.ds(a, b - a)]
                group.append(remote(src, dst, device))
            gu_copies.append(group)
        wait_all(ss_copies)
        total = ss_send[k]
        for o in kv_order:
            total = total + ss_recv[o - 1]
        scale = row_scale(total)
        h_copies = []
        for (a, b), group in zip(fspans, gu_copies):
            wait_all(group)
            gate = gu_send[k, 0, :, a:b].astype(F32)
            up = gu_send[k, 1, :, a:b].astype(F32)
            for o in kv_order:
                gate = gate + gu_recv[o - 1, 0, :, a:b].astype(F32)
                up = up + gu_recv[o - 1, 1, :, a:b].astype(F32)
            h_all[k, :, a:b] = (silu(scale * gate) * (scale * up)).astype(BF16)
            mine = h_all.at[k] if b - a == F else h_all.at[k, :, pl.ds(a, b - a)]
            h_copies.append([remote(mine, mine, kv_peer(o)[1]) for o in kv_order])
        down_load.wait()
        acc = None
        for (a, b), group in zip(fspans, h_copies):
            wait_all(group)
            part = jnp.dot(
                h_all[:, :, a:b].reshape(B, b - a),
                ref[p + "d_v"][a:b, :],
                preferred_element_type=F32,
            )
            acc = part if acc is None else acc + part
        return acc

    def scatter_rows(p, value):
        send, recv = ref[p + "_send"], ref[p + "_recv"]
        send[...] = value.astype(BF16).reshape(R, mr, d)
        copies = []
        for o in range(1, R):
            t, device = row_peer(o)
            copies.append(remote(send.at[t], recv.at[o - 1], device))
        wait_all(copies)
        total = send[r].astype(F32)
        for o in range(1, R):
            total = total + recv[o - 1].astype(F32)
        return total

    x_copies = gather_rows(ref["x"], ref["x_all"])
    own_x.wait()
    load_g1.wait()
    wait_all(x_copies)
    share = scatter_rows("p1", mixer("l", ref["x_all"], ref["g1_v"], lead))
    after = (ref["x_all"][r].astype(F32) + 0.5 * share).astype(BF16)
    ref["a_all"][r] = after
    a_copies = gather_rows(ref["a_all"].at[r], ref["a_all"])
    for copy in load_attn:
        copy.wait()
    wait_all(a_copies)

    squares = normalised(ref["a_all"], ref["g2_v"])
    f_send, f_recv = ref["f_send"], ref["f_recv"]
    q_send, q_recv = ref["q_send"], ref["q_recv"]
    v_send, v_recv = ref["v_send"], ref["v_recv"]

    def project(name):
        return jnp.dot(ref["scaled"][...], ref[name + "_v"][...], preferred_element_type=F32)

    f_send[:, :, Wp:] = squares
    f_send[:, :, :W] = project("wf").reshape(K, mk, W)
    f_copies, q_copies, v_copies = [], [], []
    for o in kv_order:
        t, device = kv_peer(o)
        f_copies.append(remote(f_send.at[t], f_recv.at[o - 1], device))
    q_send[:, 0, :, :W] = project("wq").astype(BF16).reshape(K, mk, W)
    q_send[:, 1, :, :W] = project("wk").astype(BF16).reshape(K, mk, W)
    for o in kv_order:
        t, device = kv_peer(o)
        q_copies.append(remote(q_send.at[t], q_recv.at[o - 1], device))
    v_send[:, 0] = project("wv").astype(BF16).reshape(K, mk, V)
    v_send[:, 1] = project("wg").astype(BF16).reshape(K, mk, V)
    for o in kv_order:
        t, device = kv_peer(o)
        v_copies.append(remote(v_send.at[t], v_recv.at[o - 1], device))
    for copy in load_state:
        copy.wait()
    wait_all(f_copies)
    forget = f_send[k]
    for o in kv_order:
        forget = forget + f_recv[o - 1]
    scale = row_scale(forget[:, Wp:])
    forget = scale * forget[:, :W]
    decay = jnp.exp(
        (jnp.minimum(forget, 0.0) - jnp.log1p(jnp.exp(-jnp.abs(forget)))) / 16.0 + ref["eld_v"][...]
    )
    columns = ref["columns"]
    columns[0] = decay.T
    wait_all(q_copies)
    pair = []
    for i in range(2):
        total = q_send[k, i, :, :W].astype(F32)
        for o in kv_order:
            total = total + q_recv[o - 1, i, :, :W].astype(F32)
        pair.append(scale * total)
    columns[1] = pair[1].T
    columns[2] = (pair[0] * KEY_CHANNELS ** (-0.5)).T
    wait_all(v_copies)
    pair = []
    for i in range(2):
        total = v_send[k, i].astype(F32)
        for o in kv_order:
            total = total + v_recv[o - 1, i].astype(F32)
        pair.append(scale * total)
    ref["vals"][...] = pair[0]
    gates = silu(pair[1])
    for b in range(mk):
        for h in range(heads):
            rows = slice(h * KEY_CHANNELS, (h + 1) * KEY_CHANNELS)
            lanes = slice(h * VALUE_DIM, (h + 1) * VALUE_DIM)
            new = (
                columns[0, rows, b : b + 1] * ref["st_v"][b, h]
                + columns[1, rows, b : b + 1] * ref["vals"][b : b + 1, lanes]
            )
            ref["ns_v"][b, h] = new
            ref["read"][b : b + 1, lanes] = jnp.sum(
                columns[2, rows, b : b + 1] * new, axis=0, keepdims=True
            )
    store_state = local(ref["ns_v"], ref["new_state"])
    hr_all = ref["hr_all"]
    for h in range(heads):
        lanes = slice(h * VALUE_DIM, (h + 1) * VALUE_DIM)
        out = ref["read"][:, lanes]
        out = out * lax.rsqrt(jnp.mean(out * out, axis=1, keepdims=True) + epsilon)
        hr_all[k, :, lanes] = (out * ref["hng_v"][...] * gates[:, lanes]).astype(BF16)
    hr_copies = [remote(hr_all.at[k], hr_all.at[k], kv_peer(o)[1]) for o in kv_order]
    load_out.wait()
    wait_all(hr_copies)
    mixed = scatter_rows(
        "p2",
        jnp.dot(hr_all[...].reshape(B, V), ref["wo_v"][...], preferred_element_type=F32),
    )
    second = (ref["a_all"][r].astype(F32) + mixed).astype(BF16)
    ref["s_all"][r] = second
    s_copies = gather_rows(ref["s_all"].at[r], ref["s_all"])
    load_g3.wait()
    wait_all(s_copies)

    share = scatter_rows("p3", mixer("t", ref["s_all"], ref["g3_v"], trail))
    ref["res_v"][...] = (ref["s_all"][r].astype(F32) + 0.5 * share).astype(BF16)
    store_result = local(ref["res_v"], ref["result"])
    for copy in pending:
        copy.wait_send()
    store_state.wait()
    store_result.wait()


ARGS = ("x", "st", "eld", "g1", "lg", "lu", "ld", "g2", "wq", "wk")
ARGS += ("wv", "wg", "wf", "hng", "wo", "g3", "tg", "tu", "td")


def per_device(sizes, *arrays):
    dp, tp, K = sizes
    R = dp * tp
    ref = dict(zip(ARGS, arrays))
    for n in ("g1", "g2", "g3", "hng"):
        ref[n] = ref[n].reshape(1, -1)
    mr, d = ref["x"].shape
    B, D = mr * R, d * K
    mk = B // K
    F = ref["lg"].shape[1]
    W, V = ref["wq"].shape[1], ref["wv"].shape[1]
    heads = W // KEY_CHANNELS
    Wp = padded(W)
    dims = (R, K, tp, D, B, d, F, W, V, heads)
    vm = {}
    for n in ARGS:
        if n != "x":
            vm[n + "_v"] = (ref[n].shape, ref[n].dtype)
    for n in ("x_all", "a_all", "s_all"):
        vm[n] = ((R, mr, d), BF16)
    vm["scaled"] = ((B, d), BF16)
    for p in ("l", "t"):
        vm[p + "gu_send"] = ((K, 2, mk, F), BF16)
        vm[p + "gu_recv"] = ((K - 1, 2, mk, F), BF16)
        vm[p + "ss_send"] = ((K, mk, LANES), F32)
        vm[p + "ss_recv"] = ((K - 1, mk, LANES), F32)
        vm[p + "h_all"] = ((K, mk, F), BF16)
    for p in ("p1", "p2", "p3"):
        vm[p + "_send"] = ((R, mr, d), BF16)
        vm[p + "_recv"] = ((R - 1, mr, d), BF16)
    vm["f_send"] = ((K, mk, Wp + LANES), F32)
    vm["f_recv"] = ((K - 1, mk, Wp + LANES), F32)
    vm["q_send"] = ((K, 2, mk, Wp), BF16)
    vm["q_recv"] = ((K - 1, 2, mk, Wp), BF16)
    vm["v_send"] = ((K, 2, mk, V), BF16)
    vm["v_recv"] = ((K - 1, 2, mk, V), BF16)
    vm["columns"] = ((3, W, mk), F32)
    vm["vals"] = ((mk, V), F32)
    vm["read"] = ((mk, V), F32)
    vm["ns_v"] = (ref["st"].shape, F32)
    vm["hr_all"] = ((K, mk, V), BF16)
    vm["res_v"] = ((mr, d), BF16)
    names = [*ARGS, "result", "new_state", *vm, "local_sem", "send_sem", "recv_sem"]
    sems = 3 * 2 * R + 2 * K * (1 + 2 * CHUNKS) + 4 * K
    return pl.pallas_call(
        functools.partial(kernel, dims, names),
        out_shape=(
            jax.ShapeDtypeStruct((mr, d), BF16),
            jax.ShapeDtypeStruct(ref["st"].shape, F32),
        ),
        in_specs=[pl.BlockSpec(memory_space=pl.ANY)] * len(ARGS),
        out_specs=[pl.BlockSpec(memory_space=pl.ANY)] * 2,
        scratch_shapes=[
            *[pltpu.VMEM(shape, dtype) for shape, dtype in vm.values()],
            pltpu.SemaphoreType.DMA((20 + 6 * CHUNKS,)),
            pltpu.SemaphoreType.DMA((sems,)),
            pltpu.SemaphoreType.DMA((sems,)),
        ],
        compiler_params=pltpu.CompilerParams(
            collective_id=0, has_side_effects=True, vmem_limit_bytes=63 * 1024 * 1024
        ),
    )(*[ref[n] for n in ARGS])


def solution(mesh):
    sizes = (mesh.shape["dp"], mesh.shape["tp"], mesh.shape["kv"])
    return jax.shard_map(
        functools.partial(per_device, sizes),
        mesh=mesh,
        in_specs=(
            P(("grp", "dp", "tp"), "kv"),
            P(("grp", "kv"), ("dp", "tp"), None, None),
            P(("grp", "kv"), ("dp", "tp")),
            P("kv"),
            P("kv", ("dp", "tp")),
            P("kv", ("dp", "tp")),
            P(("dp", "tp"), "kv"),
            P("kv"),
            P("kv", ("dp", "tp")),
            P("kv", ("dp", "tp")),
            P("kv", ("dp", "tp")),
            P("kv", ("dp", "tp")),
            P("kv", ("dp", "tp")),
            P(),
            P(("dp", "tp"), "kv"),
            P("kv"),
            P("kv", ("dp", "tp")),
            P("kv", ("dp", "tp")),
            P(("dp", "tp"), "kv"),
        ),
        out_specs=(P(("grp", "dp", "tp"), "kv"), P(("grp", "kv"), ("dp", "tp"), None, None)),
        check_vma=False,
    )
```

profile of v0, /device:TPU:0, one launch (start us, length us, event | category | flops | bytes accessed | tf_op | source)
XLA Modules:
  0.0 99.1 jit_solution(3009337159403054013)
XLA Ops:
  0.6 93.9 %shard_map.194 = (bf16[16,1024]{1,0:T(8,128)(2,1)}, f32[16,4,64,128]{3,2,1,0:T(8,128)}) custom-call(bf16[16,1024]{1,0:T(8,128)(2,1)} %refs_0_.1, f32[16,4,64,128]{3,2,1,0:T(8,128)} %refs_1_.1, f32[16,256]{1,0:T(8,128)} %refs_2_.1, f32[1,1024]{1,0:T(1,128)} %bitcast.4, bf16[1024,2816]{1,0:T(8,128)(2,1)} %refs_4_.1, bf16[1024,2816]{1,0:T(8,128)(2,1)} %refs_5_.1, ...), custom_call_target="tpu_custom_call" | custom-call | tf_op jit(solution)/shard_map/pallas_call | solution.py:351
  94.6 1.4 %copy.23 = bf16[16,1024]{1,0:T(8,128)(2,1)} copy(bf16[16,1024]{1,0:T(8,128)(2,1)} %get-tuple-element.4) | data formatting | bytes 65536
  96.0 3.2 %copy.24 = f32[16,4,64,128]{3,2,1,0:T(8,128)} copy(f32[16,4,64,128]{3,2,1,0:T(8,128)} %get-tuple-element.5) | data formatting | bytes 4194304
where the time goes:
time: 99.3 us; the launch traced here: 99.1 us
  Pallas kernels  93.9 us (95%)
  local copies, waits for them, and re-layouts  4.53 us (5%)
    pallas_call x1, Pallas kernels, per_device(): pl.pallas_call(functools.partial(kernel, dims, names), out_shape=(jax.Sha...  93.9 us
    unnamed x2, local copies, waits for them, and re-layouts  4.53 us

commit v1 on v0

--- a/solution.py
+++ b/solution.py
@@ -15,6 +15,9 @@
 F32 = jnp.float32
 BF16 = jnp.bfloat16
 CHUNKS = 4
+PAIRS = 4
+RELAYED_SUMS = (0, 1)
+RELAYED_HIDDEN = (0, 1)
 
 
 def spans(width, count):
@@ -37,14 +40,24 @@
 
 def kernel(dims, names, *refs):
     R, K, TP, D, B, d, F, W, V, heads = dims
-    mr, mk = B // R, B // K
+    mr, mk, DP = B // R, B // K, R // TP
     ref = dict(zip(names, refs))
     dp_i, tp_i, k = lax.axis_index("dp"), lax.axis_index("tp"), lax.axis_index("kv")
     r = dp_i * TP + tp_i
     Wp = padded(W)
     kv_order = sorted(range(1, K), key=lambda o: abs(2 * o - K))
-    counter = {"send": 0, "local": 0}
+    counter = {"send": 0, "recv": 0, "local": 0}
     pending = []
+    inner_pending, outer_pending = [], []
+    paired = K == PAIRS
+    if paired:
+        side = k // 2
+        partner = k + 1 - 2 * lax.rem(k, 2)
+        near, far = 2 - side, 3 * (1 - side)
+        across = 2 * (1 - side)
+        inner = lax.rem(k + 1, K) // 2 == 1
+        outer = jnp.logical_not(inner)
+        slot = jnp.where(inner, 1, 2)
 
     def row_peer(o):
         t = lax.rem(r + o, R)
@@ -61,20 +74,40 @@
         copy.start()
         return copy
 
-    def remote(src, dst, device):
+    def reserve(count):
+        i = counter["recv"]
+        counter["recv"] += count
+        return i
+
+    def described(src, dst, device, arrival, held):
         i = counter["send"]
         counter["send"] += 1
         copy = pltpu.make_async_remote_copy(
             src_ref=src,
             dst_ref=dst,
             send_sem=ref["send_sem"].at[i],
-            recv_sem=ref["recv_sem"].at[i],
+            recv_sem=ref["recv_sem"].at[arrival],
             device_id=device,
             device_id_type=MESH,
         )
+        held.append(copy)
+        return copy
+
+    def remote(src, dst, device, arrival=None):
+        arrival = reserve(1) if arrival is None else arrival
+        copy = described(src, dst, device, arrival, pending)
         copy.start()
-        pending.append(copy)
         return copy
+
+    def arrived(dst, arrival):
+        pltpu.make_async_remote_copy(
+            src_ref=dst,
+            dst_ref=dst,
+            send_sem=ref["send_sem"].at[0],
+            recv_sem=ref["recv_sem"].at[arrival],
+            device_id={"kv": partner},
+            device_id_type=MESH,
+        ).wait_recv()
 
     own_x = local(ref["x"], ref["x_all"].at[r])
     load_g1 = local(ref["g1"], ref["g1_v"])
@@ -123,7 +156,7 @@
     def row_scale(total):
         return lax.rsqrt(total / D + epsilon)[:, :1]
 
-    def mixer(p, buf, gain, loads):
+    def mixer_direct(p, buf, gain, loads):
         gu_loads, down_load = loads
         gu_send, gu_recv = ref[p + "gu_send"], ref[p + "gu_recv"]
         ss_send, ss_recv = ref[p + "ss_send"], ref[p + "ss_recv"]
@@ -179,6 +212,121 @@
             acc = part if acc is None else acc + part
         return acc
 
+    def part(buf, i, a, b):
+        return buf.at[i] if b - a == F else buf.at[i, :, :, pl.ds(a, b - a)]
+
+    def mixer_paired(p, buf, gain, loads):
+        gu_loads, down_load = loads
+        gu_f, gu_send, gu_recv = ref["gu_f"], ref[p + "gu_send"], ref[p + "gu_recv"]
+        relay = ref[p + "relay"]
+        ss_send, ss_recv = ref[p + "ss_send"], ref[p + "ss_recv"]
+        h_all = ref[p + "h_all"]
+        ss_send[...] = normalised(buf, gain)
+        ss_copies = []
+        for o in kv_order:
+            t, device = kv_peer(o)
+            ss_copies.append(remote(ss_send.at[t], ss_recv.at[o - 1], device))
+        sums, relays, hiddens = [], [], []
+        for c, ((a, b), pair) in enumerate(zip(fspans, gu_loads)):
+            for i, name in enumerate("gu"):
+                pair[i].wait()
+                product = jnp.dot(
+                    ref["scaled"][...], ref[p + name + "_v"][:, a:b], preferred_element_type=F32
+                ).reshape(K, mk, b - a)
+                gu_f[:, i, :, a:b] = product
+                gu_send[:, i, :, a:b] = product.astype(BF16)
+            sums.append(reserve(3))
+            relays.append(reserve(1) if c in RELAYED_SUMS else None)
+            if c in RELAYED_SUMS:
+                cut = (pl.ds(across, 2), slice(None), slice(None), pl.ds(a, b - a))
+                where = (slice(None), slice(None), slice(None), pl.ds(a, b - a))
+                copy = described(
+                    gu_send.at[cut], relay.at[where], {"kv": partner}, relays[c], outer_pending
+                )
+                pl.when(outer)(copy.start)
+            else:
+                for t in (far, near):
+                    remote(
+                        part(gu_send, t, a, b),
+                        part(gu_recv, slot, a, b),
+                        {"kv": t},
+                        sums[c] + slot,
+                    )
+            remote(part(gu_send, partner, a, b), part(gu_recv, 0, a, b), {"kv": partner}, sums[c])
+
+        relayed = []
+        for c, (a, b) in enumerate(fspans):
+            if c not in RELAYED_SUMS:
+                continue
+            onward = [
+                described(
+                    part(gu_send, t, a, b),
+                    part(gu_recv, 1, a, b),
+                    {"kv": t},
+                    sums[c] + 1,
+                    inner_pending,
+                )
+                for t in (far, near)
+            ]
+            relayed.append((c, a, b, onward))
+
+        @pl.when(inner)
+        def _():
+            for c, a, b, onward in relayed:
+                where = (slice(None), slice(None), slice(None), pl.ds(a, b - a))
+                arrived(relay.at[where], relays[c])
+                both = gu_f[pl.ds(across, 2), :, :, a:b] + relay[:, :, :, a:b].astype(F32)
+                gu_send[pl.ds(across, 2), :, :, a:b] = both.astype(BF16)
+                for copy in onward:
+                    copy.start()
+
+        wait_all(ss_copies)
+        total = ss_send[k]
+        for o in kv_order:
+            total = total + ss_recv[o - 1]
+        scale = row_scale(total)
+        for c, (a, b) in enumerate(fspans):
+            gate, up = gu_f[k, 0, :, a:b], gu_f[k, 1, :, a:b]
+            for i in (0, 1) if c in RELAYED_SUMS else (0, 1, 2):
+                arrived(part(gu_recv, i, a, b), sums[c] + i)
+                gate = gate + gu_recv[i, 0, :, a:b].astype(F32)
+                up = up + gu_recv[i, 1, :, a:b].astype(F32)
+            h_all[k, :, a:b] = (silu(scale * gate) * (scale * up)).astype(BF16)
+            mine = h_all.at[k, :, pl.ds(a, b - a)]
+            hiddens.append(reserve(3))
+            for t in (near,) if c in RELAYED_HIDDEN else (far, near):
+                remote(mine, mine, {"kv": t}, hiddens[c] + slot)
+            remote(mine, mine, {"kv": partner}, hiddens[c])
+        down_load.wait()
+        acc = None
+        for c, (a, b) in enumerate(fspans):
+            blocks = [h_all.at[i, :, pl.ds(a, b - a)] for i in (partner, near, far)]
+            for i in (1, 2):
+                arrived(blocks[i], hiddens[c] + i)
+            if c in RELAYED_HIDDEN:
+                copies = [
+                    described(
+                        blocks[i], blocks[i], {"kv": partner}, hiddens[c] + i, inner_pending
+                    )
+                    for i in (1, 2)
+                ]
+
+                @pl.when(inner)
+                def _():
+                    for copy in copies:
+                        copy.start()
+
+            arrived(blocks[0], hiddens[c])
+            product = jnp.dot(
+                h_all[:, :, a:b].reshape(B, b - a),
+                ref[p + "d_v"][a:b, :],
+                preferred_element_type=F32,
+            )
+            acc = product if acc is None else acc + product
+        return acc
+
+    mixer = mixer_paired if paired else mixer_direct
+
     def scatter_rows(p, value):
         send, recv = ref[p + "_send"], ref[p + "_recv"]
         send[...] = value.astype(BF16).reshape(R, mr, d)
@@ -192,17 +340,45 @@
             total = total + recv[o - 1].astype(F32)
         return total
 
+    def reduce_rows_twice(p, value, buf, factor, out):
+        total = scatter_rows(p, value)
+        out[r] = (buf[r].astype(F32) + factor * total).astype(BF16)
+        wait_all(gather_rows(out.at[r], out))
+
+    def reduce_rows_once(p, value, buf, factor, out):
+        whole, send, recv, parts = ref["rows_f"], ref[p + "_send"], ref[p + "_recv"], ref[p + "_parts"]
+        whole[...] = value.reshape(DP, TP, mr, d)
+        firsts, seconds = [], []
+        spans_d = spans(d, 2)
+        for a, b in spans_d:
+            send[:, :, a:b] = whole[:, 1 - tp_i, :, a:b].astype(BF16)
+            cut = (slice(None), slice(None), pl.ds(a, b - a))
+            firsts.append(remote(send.at[cut], recv.at[cut], {"tp": 1 - tp_i}))
+        for (a, b), first in zip(spans_d, firsts):
+            first.wait_recv()
+            chip = whole[:, tp_i, :, a:b] + recv[:, :, a:b].astype(F32)
+            parts[dp_i, tp_i, :, :, a:b] = chip.astype(BF16)
+            mine = parts.at[dp_i, tp_i, :, :, pl.ds(a, b - a)]
+            for o in sorted(range(1, R), key=lambda o: o % TP == 0):
+                seconds.append(remote(mine, mine, row_peer(o)[1]))
+        wait_all(seconds)
+        for j in range(DP):
+            for c in range(TP):
+                total = parts[0, c, j].astype(F32)
+                for x in range(1, DP):
+                    total = total + parts[x, c, j].astype(F32)
+                i = j * TP + c
+                out[i] = (buf[i].astype(F32) + factor * total).astype(BF16)
+
+    reduce_rows = reduce_rows_once if DP == 2 and TP == 2 else reduce_rows_twice
+
     x_copies = gather_rows(ref["x"], ref["x_all"])
     own_x.wait()
     load_g1.wait()
     wait_all(x_copies)
-    share = scatter_rows("p1", mixer("l", ref["x_all"], ref["g1_v"], lead))
-    after = (ref["x_all"][r].astype(F32) + 0.5 * share).astype(BF16)
-    ref["a_all"][r] = after
-    a_copies = gather_rows(ref["a_all"].at[r], ref["a_all"])
+    reduce_rows("p1", mixer("l", ref["x_all"], ref["g1_v"], lead), ref["x_all"], 0.5, ref["a_all"])
     for copy in load_attn:
         copy.wait()
-    wait_all(a_copies)
 
     squares = normalised(ref["a_all"], ref["g2_v"])
     f_send, f_recv = ref["f_send"], ref["f_recv"]
@@ -267,11 +443,10 @@
                 columns[0, rows, b : b + 1] * ref["st_v"][b, h]
                 + columns[1, rows, b : b + 1] * ref["vals"][b : b + 1, lanes]
             )
-            ref["ns_v"][b, h] = new
+            ref["new_state"][b, h] = new
             ref["read"][b : b + 1, lanes] = jnp.sum(
                 columns[2, rows, b : b + 1] * new, axis=0, keepdims=True
             )
-    store_state = local(ref["ns_v"], ref["new_state"])
     hr_all = ref["hr_all"]
     for h in range(heads):
         lanes = slice(h * VALUE_DIM, (h + 1) * VALUE_DIM)
@@ -281,23 +456,25 @@
     hr_copies = [remote(hr_all.at[k], hr_all.at[k], kv_peer(o)[1]) for o in kv_order]
     load_out.wait()
     wait_all(hr_copies)
-    mixed = scatter_rows(
-        "p2",
-        jnp.dot(hr_all[...].reshape(B, V), ref["wo_v"][...], preferred_element_type=F32),
-    )
-    second = (ref["a_all"][r].astype(F32) + mixed).astype(BF16)
-    ref["s_all"][r] = second
-    s_copies = gather_rows(ref["s_all"].at[r], ref["s_all"])
+    mixed = jnp.dot(hr_all[...].reshape(B, V), ref["wo_v"][...], preferred_element_type=F32)
+    reduce_rows("p2", mixed, ref["a_all"], 1.0, ref["s_all"])
     load_g3.wait()
-    wait_all(s_copies)
 
     share = scatter_rows("p3", mixer("t", ref["s_all"], ref["g3_v"], trail))
-    ref["res_v"][...] = (ref["s_all"][r].astype(F32) + 0.5 * share).astype(BF16)
-    store_result = local(ref["res_v"], ref["result"])
+    ref["result"][...] = (ref["s_all"][r].astype(F32) + 0.5 * share).astype(BF16)
     for copy in pending:
         copy.wait_send()
-    store_state.wait()
-    store_result.wait()
+    if paired:
+
+        @pl.when(inner)
+        def _():
+            for copy in inner_pending:
+                copy.wait_send()
+
+        @pl.when(outer)
+        def _():
+            for copy in outer_pending:
+                copy.wait_send()
 
 
 ARGS = ("x", "st", "eld", "g1", "lg", "lu", "ld", "g2", "wq", "wk")
@@ -331,9 +508,21 @@
         vm[p + "ss_send"] = ((K, mk, LANES), F32)
         vm[p + "ss_recv"] = ((K - 1, mk, LANES), F32)
         vm[p + "h_all"] = ((K, mk, F), BF16)
+        if K == PAIRS:
+            vm[p + "relay"] = ((2, 2, mk, F), BF16)
+    if K == PAIRS:
+        vm["gu_f"] = ((K, 2, mk, F), F32)
+    once = dp == 2 and tp == 2
+    if once:
+        vm["rows_f"] = ((dp, tp, mr, d), F32)
     for p in ("p1", "p2", "p3"):
-        vm[p + "_send"] = ((R, mr, d), BF16)
-        vm[p + "_recv"] = ((R - 1, mr, d), BF16)
+        if once and p != "p3":
+            vm[p + "_send"] = ((dp, mr, d), BF16)
+            vm[p + "_recv"] = ((dp, mr, d), BF16)
+            vm[p + "_parts"] = ((dp, tp, dp, mr, d), BF16)
+        else:
+            vm[p + "_send"] = ((R, mr, d), BF16)
+            vm[p + "_recv"] = ((R - 1, mr, d), BF16)
     vm["f_send"] = ((K, mk, Wp + LANES), F32)
     vm["f_recv"] = ((K - 1, mk, Wp + LANES), F32)
     vm["q_send"] = ((K, 2, mk, Wp), BF16)
@@ -343,19 +532,17 @@
     vm["columns"] = ((3, W, mk), F32)
     vm["vals"] = ((mk, V), F32)
     vm["read"] = ((mk, V), F32)
-    vm["ns_v"] = (ref["st"].shape, F32)
     vm["hr_all"] = ((K, mk, V), BF16)
-    vm["res_v"] = ((mr, d), BF16)
     names = [*ARGS, "result", "new_state", *vm, "local_sem", "send_sem", "recv_sem"]
-    sems = 3 * 2 * R + 2 * K * (1 + 2 * CHUNKS) + 4 * K
+    sems = 4 * 2 * R + 2 * K * (1 + 3 * CHUNKS) + 4 * K
     return pl.pallas_call(
         functools.partial(kernel, dims, names),
         out_shape=(
-            jax.ShapeDtypeStruct((mr, d), BF16),
-            jax.ShapeDtypeStruct(ref["st"].shape, F32),
+            pltpu.VMEM((mr, d), BF16),
+            pltpu.VMEM(ref["st"].shape, F32),
         ),
         in_specs=[pl.BlockSpec(memory_space=pl.ANY)] * len(ARGS),
-        out_specs=[pl.BlockSpec(memory_space=pl.ANY)] * 2,
+        out_specs=[pl.BlockSpec(memory_space=pltpu.VMEM)] * 2,
         scratch_shapes=[
             *[pltpu.VMEM(shape, dtype) for shape, dtype in vm.values()],
             pltpu.SemaphoreType.DMA((20 + 6 * CHUNKS,)),
@@ -363,7 +550,7 @@
             pltpu.SemaphoreType.DMA((sems,)),
         ],
         compiler_params=pltpu.CompilerParams(
-            collective_id=0, has_side_effects=True, vmem_limit_bytes=63 * 1024 * 1024
+            collective_id=0, has_side_effects=True, vmem_limit_bytes=56 * 1024 * 1024
         ),
     )(*[ref[n] for n in ARGS])
 

time: 99.3 us -> 90.2 us (0.908)
  Pallas kernels: 93.9 us -> 87.5 us
  local copies, waits for them, and re-layouts: 4.53 us -> 1.94 us
    pallas_call x1, Pallas kernels: 93.9 us -> 87.5 us  [per_device(): pl.pallas_call(functools.partial(kernel, dims, names), out_shape=(pltpu.V...]
    unnamed x2, local copies, waits for them, and re-layouts: 4.53 us -> 1.94 us
where the time goes in v1:
time: 90.2 us; the launch traced here: 90 us
  Pallas kernels  87.5 us (97%)
  local copies, waits for them, and re-layouts  1.94 us (2%)
    pallas_call x1, Pallas kernels, per_device(): pl.pallas_call(functools.partial(kernel, dims, names), out_shape=(pltpu.V...  87.5 us
    unnamed x2, local copies, waits for them, and re-layouts  1.94 us

profile of v1, /device:TPU:0, one launch (start us, length us, event | category | flops | bytes accessed | tf_op | source)
XLA Modules:
  0.0 90.0 jit_solution(7728931604548671070)
XLA Ops:
  0.6 87.5 %shard_map.194 = (bf16[16,1024]{1,0:T(8,128)(2,1)S(1)}, f32[16,4,64,128]{3,2,1,0:T(8,128)S(1)}) custom-call(bf16[16,1024]{1,0:T(8,128)(2,1)} %refs_0_.1, f32[16,4,64,128]{3,2,1,0:T(8,128)} %refs_1_.1, f32[16,256]{1,0:T(8,128)} %refs_2_.1, f32[1,1024]{1,0:T(1,128)} %bitcast.4, bf16[1024,2816]{1,0:T(8,128)(2,1)} %refs_4_.1, bf16[1024,2816]{1,0:T(8,128)(2,1)} %refs_5_.1, ...), custom_call_target="tpu_custom_call" | custom-call | tf_op jit(solution)/shard_map/pallas_call | solution.py:538
  88.1 0.6 copy.23
  88.7 1.3 %copy.24 = f32[16,4,64,128]{3,2,1,0:T(8,128)} copy(f32[16,4,64,128]{3,2,1,0:T(8,128)S(1)} %get-tuple-element.3) | data formatting | bytes 4194304

commit v2 on v0

v2 whole, which is shorter than its diff:
```python
import functools

import jax
import jax.numpy as jnp
from jax import lax
from jax.experimental import pallas as pl
from jax.experimental.pallas import tpu as pltpu
from jax.sharding import PartitionSpec as P

KEY_CHANNELS = 64
VALUE_DIM = 128
LANES = 128
epsilon = 1e-06
MESH = pl.DeviceIdType.MESH
F32 = jnp.float32
BF16 = jnp.bfloat16
CHUNKS = 4
PAIRS = 4
SHARES = (3, 4, 4)
RELAYED_SUMS = (3, 3)
RELAYED_HIDDEN = ((0, 1), ())
FIRST = (8.9, 9.8, 10.9, 13.0, 14.0, 16.0, 17.0, 19.0, 22.0, 23.0, 25.0, 28.0, 30.0, 32.0)
FIRST += (33.0, 33.1, 35.0, 38.0, 39.0, 40.0, 41.0, 43.0, 44.0, 44.1, 49.0, 50.0, 52.0, 54.0)
FIRST += (54.1, 54.2, 55.0, 57.0, 59.0, 62.0, 64.0, 67.0, 69.0, 71.0, 74.0)
SECOND = (15.0, 18.0, 20.0, 21.0, 24.0, 26.0, 27.0, 33.2, 33.3, 36.0, 36.1, 36.2, 37.0, 37.1)
SECOND += (42.0, 45.0, 46.0, 47.0, 48.0, 51.0, 53.0, 53.1, 56.0, 58.0, 60.0, 61.0, 63.0, 65.0)
SECOND += (66.0, 71.1, 71.2, 73.0, 73.1, 73.2, 75.0)
READY = (FIRST, SECOND)


def spans(width, count):
    if width % LANES:
        return [(0, width)]
    tile = 2 * LANES if width % (2 * LANES) == 0 else LANES
    tiles = width // tile
    count = min(count, tiles)
    cuts = [tile * ((tiles * i + count - 1) // count) for i in range(count + 1)]
    return list(zip(cuts[:-1], cuts[1:]))


def shared(width, shares):
    tile = 2 * LANES
    tiles = width // tile
    if width % tile or tiles < sum(shares):
        return spans(width, len(shares))
    ends = [sum(shares[: i + 1]) for i in range(len(shares))]
    cuts = [0] + [tile * (tiles * end // sum(shares)) for end in ends]
    return list(zip(cuts[:-1], cuts[1:]))


def padded(width):
    return -(-width // LANES) * LANES


def silu(x):
    return x * jax.nn.sigmoid(x)


def kernel(dims, names, *refs):
    R, K, TP, D, B, d, F, W, V, heads, S = dims
    DP = R // TP
    rows, hr, hm = B // S, B // R // S, B // K // S
    ref = dict(zip(names, refs))
    dp_i, tp_i, k = lax.axis_index("dp"), lax.axis_index("tp"), lax.axis_index("kv")
    r = dp_i * TP + tp_i
    Wp = padded(W)
    kv_order = sorted(range(1, K), key=lambda o: abs(2 * o - K))
    counter = {"send": 0, "recv": 0, "local": 0}
    pending, inner_pending, outer_pending = [], [], []
    waited = set()
    paired = K == PAIRS
    if paired:
        side = k // 2
        partner = k + 1 - 2 * lax.rem(k, 2)
        near, far = 2 - side, 3 * (1 - side)
        across = 2 * (1 - side)
        inner = lax.rem(k + 1, K) // 2 == 1
        outer = jnp.logical_not(inner)
        slot = jnp.where(inner, 1, 2)

    def row_peer(o):
        t = lax.rem(r + o, R)
        return t, {"dp": t // TP, "tp": lax.rem(t, TP)}

    def kv_peer(o):
        t = lax.rem(k + o, K)
        return t, {"kv": t}

    def local(src, dst):
        i = counter["local"]
        counter["local"] += 1
        copy = pltpu.make_async_copy(src, dst, ref["local_sem"].at[i])
        copy.start()
        return copy

    def loaded(*copies):
        for copy in copies:
            if id(copy) not in waited:
                waited.add(id(copy))
                copy.wait()

    def group():
        pair = counter["send"], counter["recv"]
        counter["send"] += 1
        counter["recv"] += 1
        return pair

    def arrival():
        counter["recv"] += 1
        return counter["recv"] - 1

    def described(src, dst, device, sems):
        return pltpu.make_async_remote_copy(
            src_ref=src,
            dst_ref=dst,
            send_sem=ref["send_sem"].at[sems[0]],
            recv_sem=ref["recv_sem"].at[sems[1]],
            device_id=device,
            device_id_type=MESH,
        )

    def remote(src, dst, device, sems):
        described(src, dst, device, sems).start()

    def arrived(block, sems):
        described(block, block, row_peer(1)[1], (0, sems[1])).wait_recv()

    def left(block, sems):
        described(block, block, row_peer(1)[1], (sems[0], 0)).wait_send()

    def to_kv_peers(block_of, recv, like):
        sems = group()
        for o in kv_order:
            t, device = kv_peer(o)
            remote(block_of(t), recv(o), device, sems)
        pending.append((like, sems))
        return sems

    own_x = [local(ref["x"].at[pl.ds(s * hr, hr)], ref["x_all", s].at[r]) for s in range(S)]
    load_g1 = local(ref["g1"], ref["g1_v"])
    fspans = shared(F, SHARES) if paired else spans(F, CHUNKS)

    def load_mixer(p):
        first = []
        for a, b in fspans:
            cut = (slice(None), slice(None)) if b - a == F else (slice(None), pl.ds(a, b - a))
            first.append(
                (
                    local(ref[p + "g"].at[cut], ref[p + "g_v"].at[cut]),
                    local(ref[p + "u"].at[cut], ref[p + "u_v"].at[cut]),
                )
            )
        return first, local(ref[p + "d"], ref[p + "d_v"])

    lead = load_mixer("l")
    load_attn = [local(ref[n], ref[n + "_v"]) for n in ("g2", "wq", "wk", "wf", "wv", "wg")]
    load_state = [local(ref[n], ref[n + "_v"]) for n in ("st", "eld", "hng")]
    load_out = local(ref["wo"], ref["wo_v"])
    load_g3 = local(ref["g3"], ref["g3_v"])
    trail = load_mixer("t")

    barrier = pltpu.get_barrier_semaphore()
    for o in range(1, R):
        pl.semaphore_signal(barrier, inc=1, device_id=row_peer(o)[1], device_id_type=MESH)
    for o in kv_order:
        pl.semaphore_signal(barrier, inc=1, device_id=kv_peer(o)[1], device_id_type=MESH)
    pl.semaphore_wait(barrier, R - 1 + K - 1)

    def gather_rows(buf):
        sems = group()
        for o in range(1, R):
            remote(buf.at[r], buf.at[r], row_peer(o)[1], sems)
        pending.append((buf.at[pl.ds(0, R - 1)], sems))
        return sems

    def flat(block):
        if hm % 16 == 0:
            return block.reshape(rows, -1)
        return block.astype(F32).reshape(rows, -1).astype(BF16)

    def normalised(s, buf, gain):
        wide = buf[...].astype(F32).reshape(rows, d)
        squares = jnp.sum(wide * wide, axis=1, keepdims=True)
        ref["scaled", s][...] = (wide * gain[...]).astype(BF16)
        return jnp.broadcast_to(squares, (rows, LANES)).reshape(K, hm, LANES)

    def row_scale(total):
        return lax.rsqrt(total / D + epsilon)[:, :1]

    def part(buf, i, a, b):
        return buf.at[i] if b - a == F else buf.at[i, :, :, pl.ds(a, b - a)]

    def piece(buf, i, a, b):
        return buf.at[i] if b - a == F else buf.at[i, :, pl.ds(a, b - a)]

    def send_squares(p, s, buf, gain):
        ss_send, ss_recv = ref[p, "ss_send", s], ref[p, "ss_recv", s]
        ss_send[...] = normalised(s, buf, gain)
        return to_kv_peers(
            lambda t: ss_send.at[t], lambda o: ss_recv.at[o - 1], ss_send.at[pl.ds(0, K - 1)]
        )

    def total_scale(p, s, sems):
        arrived(ref[p, "ss_recv", s], sems)
        total = ref[p, "ss_send", s][k]
        for o in kv_order:
            total = total + ref[p, "ss_recv", s][o - 1]
        return row_scale(total)

    def mixer_direct(p, s, buf, gain, loads):
        gu_loads, down_load = loads
        gu_send, gu_recv, h_all = ref[p, "gu_send", s], ref[p, "gu_recv", s], ref[p, "h_all", s]
        loaded(load_g1, load_g3)
        ss_sems = send_squares(p, s, buf, gain)
        gu_sems = []
        for (a, b), pair in zip(fspans, gu_loads):
            for i, name in enumerate("gu"):
                loaded(pair[i])
                product = jnp.dot(
                    ref["scaled", s][...], ref[p + name + "_v"][:, a:b], preferred_element_type=F32
                )
                gu_send[:, i, :, a:b] = product.reshape(K, hm, b - a).astype(BF16)
            gu_sems.append(
                to_kv_peers(
                    lambda t: part(gu_send, t, a, b),
                    lambda o: part(gu_recv, o - 1, a, b),
                    part(gu_send, pl.ds(0, K - 1), a, b),
                )
            )
        scale = total_scale(p, s, ss_sems)
        h_sems = []
        for (a, b), sems in zip(fspans, gu_sems):
            arrived(part(gu_recv, pl.ds(0, K - 1), a, b), sems)
            gate = gu_send[k, 0, :, a:b].astype(F32)
            up = gu_send[k, 1, :, a:b].astype(F32)
            for o in kv_order:
                gate = gate + gu_recv[o - 1, 0, :, a:b].astype(F32)
                up = up + gu_recv[o - 1, 1, :, a:b].astype(F32)
            h_all[k, :, a:b] = (silu(scale * gate) * (scale * up)).astype(BF16)
            mine = piece(h_all, k, a, b)
            h_sems.append(
                to_kv_peers(lambda t: mine, lambda o: mine, piece(h_all, pl.ds(0, K - 1), a, b))
            )
        loaded(down_load)
        acc = None
        for (a, b), sems in zip(fspans, h_sems):
            arrived(piece(h_all, pl.ds(0, K - 1), a, b), sems)
            product = jnp.dot(
                flat(h_all[:, :, a:b]), ref[p + "d_v"][a:b, :], preferred_element_type=F32
            )
            acc = product if acc is None else acc + product
        return acc
        yield

    def mixer_paired(p, s, buf, gain, loads):
        gu_loads, down_load = loads
        gu_f, gu_send, gu_recv = ref["gu_f", s], ref[p, "gu_send", s], ref[p, "gu_recv", s]
        relay, h_all = ref[p, "relay", s], ref[p, "h_all", s]
        loaded(load_g1 if p == "l" else load_g3)
        ss_sems = send_squares(p, s, buf, gain)
        sums, relays, hiddens = [], [], [None] * len(fspans)
        relayed, forwarded = RELAYED_SUMS[s], RELAYED_HIDDEN[s]

        def to_partner(c):
            a, b = fspans[c]
            remote(part(gu_send, partner, a, b), part(gu_recv, 0, a, b), {"kv": partner}, sums[c])
            pending.append((part(gu_send, pl.ds(0, 3), a, b), sums[c]))

        for c, ((a, b), pair) in enumerate(zip(fspans, gu_loads)):
            if c:
                yield
            for i, name in enumerate("gu"):
                loaded(pair[i])
                product = jnp.dot(
                    ref["scaled", s][...], ref[p + name + "_v"][:, a:b], preferred_element_type=F32
                ).reshape(K, hm, b - a)
                gu_f[:, i, :, a:b] = product
                gu_send[:, i, :, a:b] = product.astype(BF16)
            sums.append(group())
            if c < relayed:
                relays.append(arrival())
                cut = (pl.ds(across, 2), slice(None), slice(None), pl.ds(a, b - a))
                where = (slice(None), slice(None), slice(None), pl.ds(a, b - a))
                copy = described(
                    gu_send.at[cut], relay.at[where], {"kv": partner}, (sums[c][0], relays[c])
                )
                pl.when(outer)(copy.start)
            else:
                for t in (far, near):
                    remote(
                        part(gu_send, t, a, b), part(gu_recv, slot, a, b), {"kv": t}, sums[c]
                    )
            if c:
                to_partner(c - 1)
        to_partner(len(fspans) - 1)

        def pass_on(c):
            a, b = fspans[c]
            where = (slice(None), slice(None), slice(None), pl.ds(a, b - a))
            onward = [
                described(part(gu_send, t, a, b), part(gu_recv, 1, a, b), {"kv": t}, sums[c])
                for t in (far, near)
            ]

            @pl.when(inner)
            def _():
                arrived(relay.at[where], (0, relays[c]))
                both = gu_f[pl.ds(across, 2), :, :, a:b] + relay[:, :, :, a:b].astype(F32)
                gu_send[pl.ds(across, 2), :, :, a:b] = both.astype(BF16)
                for copy in onward:
                    copy.start()

        for c in range(relayed):
            yield
            pass_on(c)
        yield
        scale = total_scale(p, s, ss_sems)
        for c, (a, b) in enumerate(fspans):
            if c:
                yield
            gate, up = gu_f[k, 0, :, a:b], gu_f[k, 1, :, a:b]
            blocks = 2 if c < relayed else 3
            arrived(part(gu_recv, pl.ds(0, blocks), a, b), sums[c])
            for i in range(blocks):
                gate = gate + gu_recv[i, 0, :, a:b].astype(F32)
                up = up + gu_recv[i, 1, :, a:b].astype(F32)
            h_all[k, :, a:b] = (silu(scale * gate) * (scale * up)).astype(BF16)
            mine = h_all.at[k, :, pl.ds(a, b - a)]
            hiddens[c] = group()
            for t in (near, partner) if c in forwarded else (far, near, partner):
                remote(mine, mine, {"kv": t}, hiddens[c])
            if c in forwarded:
                inner_pending.append((h_all.at[:, :, pl.ds(a, b - a)], hiddens[c]))
                outer_pending.append((h_all.at[pl.ds(0, 2), :, pl.ds(a, b - a)], hiddens[c]))
            else:
                pending.append((h_all.at[pl.ds(0, 3), :, pl.ds(a, b - a)], hiddens[c]))
        for c in forwarded:
            yield
            a, b = fspans[c]
            blocks = [h_all.at[i, :, pl.ds(a, b - a)] for i in (near, far)]
            copies = [described(block, block, {"kv": partner}, hiddens[c]) for block in blocks]

            @pl.when(inner)
            def _():
                arrived(h_all.at[pl.ds(0, 3), :, pl.ds(a, b - a)], hiddens[c])
                for copy in copies:
                    copy.start()

        acc = None
        for c, (a, b) in enumerate(fspans):
            yield
            loaded(down_load)
            if c in forwarded:

                @pl.when(outer)
                def _():
                    arrived(h_all.at[pl.ds(0, 3), :, pl.ds(a, b - a)], hiddens[c])

            else:
                arrived(h_all.at[pl.ds(0, 3), :, pl.ds(a, b - a)], hiddens[c])
            product = jnp.dot(
                flat(h_all[:, :, a:b]), ref[p + "d_v"][a:b, :], preferred_element_type=F32
            )
            acc = product if acc is None else acc + product
        return acc

    mixer = mixer_paired if paired else mixer_direct

    def scatter_rows(p, s, value):
        send, recv = ref[p, "_send", s], ref[p, "_recv", s]
        send[...] = value.reshape(R, hr, d).astype(BF16)
        sems = group()
        for o in range(1, R):
            t, device = row_peer(o)
            remote(send.at[t], recv.at[o - 1], device, sems)
        pending.append((send.at[pl.ds(0, R - 1)], sems))
        return sems

    def scattered(p, s, sems):
        send, recv = ref[p, "_send", s], ref[p, "_recv", s]
        arrived(recv, sems)
        total = send[r].astype(F32)
        for o in range(1, R):
            total = total + recv[o - 1].astype(F32)
        return total

    def reduce_rows_twice(p, s, value, buf, factor, out):
        total = scattered(p, s, scatter_rows(p, s, value))
        out[r] = (buf[r].astype(F32) + factor * total).astype(BF16)
        arrived(out.at[pl.ds(0, R - 1)], gather_rows(out))
        return
        yield

    def reduce_rows_once(p, s, value, buf, factor, out):
        whole, send, recv, parts = ref["rows_f", s], ref[p, "_send", s], ref[p, "_recv", s], ref[p, "_parts", s]
        whole[...] = value.reshape(DP, TP, hr, d)
        first, second = group(), group()
        halves = [first[1], arrival()]
        spans_d = spans(d, 2)
        for a, b in spans_d:
            send[:, :, a:b] = whole[:, 1 - tp_i, :, a:b].astype(BF16)
            cut = (slice(None), slice(None), pl.ds(a, b - a))
            remote(send.at[cut], recv.at[cut], {"tp": 1 - tp_i}, (first[0], halves[a > 0]))
        pending.append((send, first))
        for (a, b), half in zip(spans_d, halves):
            yield
            arrived(recv.at[:, :, pl.ds(a, b - a)], (0, half))
            chip = whole[:, tp_i, :, a:b] + recv[:, :, a:b].astype(F32)
            parts[r, :, :, a:b] = chip.astype(BF16)
            mine = parts.at[r, :, :, pl.ds(a, b - a)]
            for o in sorted(range(1, R), key=lambda o: o % TP == 0):
                remote(mine, mine, row_peer(o)[1], second)
        pending.append((parts.at[pl.ds(0, R - 1)], second))
        yield
        arrived(parts.at[pl.ds(0, R - 1)], second)
        for j in range(DP):
            for c in range(TP):
                total = parts[c, j].astype(F32)
                for x in range(1, DP):
                    total = total + parts[x * TP + c, j].astype(F32)
                i = j * TP + c
                out[i] = (buf[i].astype(F32) + factor * total).astype(BF16)

    reduce_rows = reduce_rows_once if DP == 2 and TP == 2 else reduce_rows_twice

    def chain(s):
        x_all, a_all, s_all = ref["x_all", s], ref["a_all", s], ref["s_all", s]
        loaded(own_x[s])
        sems = gather_rows(x_all)
        yield
        arrived(x_all.at[pl.ds(0, R - 1)], sems)
        mixed = yield from mixer("l", s, x_all, ref["g1_v"], lead)
        yield from reduce_rows("p1", s, mixed, x_all, 0.5, a_all)

        loaded(*load_attn)
        squares = normalised(s, a_all, ref["g2_v"])
        f_send, f_recv = ref["f_send", s], ref["f_recv", s]
        q_send, q_recv = ref["q_send", s], ref["q_recv", s]
        v_send, v_recv = ref["v_send", s], ref["v_recv", s]

        def project(name, width):
            return jnp.dot(
                ref["scaled", s][...], ref[name + "_v"][...], preferred_element_type=F32
            ).reshape(K, hm, width)

        f_send[:, :, Wp:] = squares
        f_send[:, :, :W] = project("wf", W)

        def exchange(send, recv):
            return to_kv_peers(
                lambda t: send.at[t], lambda o: recv.at[o - 1], send.at[pl.ds(0, K - 1)]
            )

        f_sems = exchange(f_send, f_recv)
        q_send[:, 0, :, :W] = project("wq", W).astype(BF16)
        q_send[:, 1, :, :W] = project("wk", W).astype(BF16)
        q_sems = exchange(q_send, q_recv)
        v_send[:, 0] = project("wv", V).astype(BF16)
        v_send[:, 1] = project("wg", V).astype(BF16)
        v_sems = exchange(v_send, v_recv)
        yield
        loaded(*load_state)
        arrived(f_recv, f_sems)
        forget = f_send[k]
        for o in kv_order:
            forget = forget + f_recv[o - 1]
        scale = row_scale(forget[:, Wp:])
        forget = scale * forget[:, :W]
        mine = slice(s * hm, (s + 1) * hm)
        decay = jnp.exp(
            (jnp.minimum(forget, 0.0) - jnp.log1p(jnp.exp(-jnp.abs(forget)))) / 16.0
            + ref["eld_v"][mine]
        )
        columns, read, vals = ref["columns", s], ref["read", s], ref["vals", s]
        columns[0] = decay.T
        yield
        arrived(q_recv, q_sems)
        pair = []
        for i in range(2):
            total = q_send[k, i, :, :W].astype(F32)
            for o in kv_order:
                total = total + q_recv[o - 1, i, :, :W].astype(F32)
            pair.append(scale * total)
        queries = pair[0] * KEY_CHANNELS ** (-0.5)
        columns[1] = pair[1].T
        columns[2] = (queries * decay).T
        overlap = queries * pair[1]
        for b in range(hm):
            for h in range(heads):
                keys = slice(h * KEY_CHANNELS, (h + 1) * KEY_CHANNELS)
                lanes = slice(h * VALUE_DIM, (h + 1) * VALUE_DIM)
                read[b : b + 1, lanes] = jnp.sum(
                    columns[2, keys, b : b + 1] * ref["st_v"][s * hm + b, h], axis=0, keepdims=True
                )
        yield
        arrived(v_recv, v_sems)
        pair = []
        for i in range(2):
            total = v_send[k, i].astype(F32)
            for o in kv_order:
                total = total + v_recv[o - 1, i].astype(F32)
            pair.append(scale * total)
        vals[...] = pair[0]
        gates = silu(pair[1])
        hr_all = ref["hr_all", s]
        for h in range(heads):
            lanes = slice(h * VALUE_DIM, (h + 1) * VALUE_DIM)
            keys = slice(h * KEY_CHANNELS, (h + 1) * KEY_CHANNELS)
            out = read[:, lanes] + (
                jnp.sum(overlap[:, keys], axis=1, keepdims=True) * pair[0][:, lanes]
            )
            out = out * lax.rsqrt(jnp.mean(out * out, axis=1, keepdims=True) + epsilon)
            hr_all[k, :, lanes] = (out * ref["hng_v"][...] * gates[:, lanes]).astype(BF16)
        hr_sems = to_kv_peers(
            lambda t: hr_all.at[k], lambda o: hr_all.at[k], hr_all.at[pl.ds(0, K - 1)]
        )
        yield
        for b in range(hm):
            for h in range(heads):
                keys = slice(h * KEY_CHANNELS, (h + 1) * KEY_CHANNELS)
                lanes = slice(h * VALUE_DIM, (h + 1) * VALUE_DIM)
                ref["new_state"][s * hm + b, h] = (
                    columns[0, keys, b : b + 1] * ref["st_v"][s * hm + b, h]
                    + columns[1, keys, b : b + 1] * vals[b : b + 1, lanes]
                )
        yield
        loaded(load_out)
        arrived(hr_all.at[pl.ds(0, K - 1)], hr_sems)
        mixed = jnp.dot(flat(hr_all[...]), ref["wo_v"][...], preferred_element_type=F32)
        yield from reduce_rows("p2", s, mixed, a_all, 1.0, s_all)

        mixed = yield from mixer("t", s, s_all, ref["g3_v"], trail)
        sems = scatter_rows("p3", s, mixed)
        yield
        share = scattered("p3", s, sems)
        ref["result"][s * hr : (s + 1) * hr] = (s_all[r].astype(F32) + 0.5 * share).astype(BF16)

    chains = [chain(s) for s in range(S)]
    taken = {}
    for s, steps in enumerate(chains):
        next(steps)
        taken[s] = 0
    while taken:
        s = min(taken, key=lambda i: READY[i][taken[i]] if S > 1 else 0)
        if next(chains[s], chains) is chains:
            del taken[s]
        else:
            taken[s] += 1
    loaded(load_g3)
    for block, sems in pending:
        left(block, sems)
    if inner_pending:

        @pl.when(inner)
        def _():
            for block, sems in inner_pending:
                left(block, sems)

        @pl.when(outer)
        def _():
            for block, sems in outer_pending:
                left(block, sems)


ARGS = ("x", "st", "eld", "g1", "lg", "lu", "ld", "g2", "wq", "wk")
ARGS += ("wv", "wg", "wf", "hng", "wo", "g3", "tg", "tu", "td")


def store(result, state, result_out, state_out, sem):
    copies = [
        pltpu.make_async_copy(state, state_out, sem.at[0]),
        pltpu.make_async_copy(result, result_out, sem.at[1]),
    ]
    for copy in copies:
        copy.start()
    for copy in copies:
        copy.wait()


def per_device(sizes, *arrays):
    dp, tp, K = sizes
    R = dp * tp
    ref = dict(zip(ARGS, arrays))
    for n in ("g1", "g2", "g3", "hng"):
        ref[n] = ref[n].reshape(1, -1)
    mr, d = ref["x"].shape
    B, D = mr * R, d * K
    F = ref["lg"].shape[1]
    W, V = ref["wq"].shape[1], ref["wv"].shape[1]
    heads = W // KEY_CHANNELS
    Wp = padded(W)
    paired = K == PAIRS
    S = 2 if paired and mr * K == B and mr % 16 == 0 else 1
    rows, hr, hm = B // S, mr // S, B // K // S
    dims = (R, K, tp, D, B, d, F, W, V, heads, S)
    once = dp == 2 and tp == 2
    vm = {}
    for n in ARGS:
        if n != "x":
            vm[n + "_v"] = (ref[n].shape, ref[n].dtype)
    for s in range(S):
        for n in ("x_all", "a_all", "s_all"):
            vm[n, s] = ((R, hr, d), BF16)
        vm["scaled", s] = ((rows, d), BF16)
        for p in ("l", "t"):
            vm[p, "gu_send", s] = ((K, 2, hm, F), BF16)
            vm[p, "gu_recv", s] = ((K - 1, 2, hm, F), BF16)
            vm[p, "ss_send", s] = ((K, hm, LANES), F32)
            vm[p, "ss_recv", s] = ((K - 1, hm, LANES), F32)
            vm[p, "h_all", s] = ((K, hm, F), BF16)
            if paired:
                vm[p, "relay", s] = ((2, 2, hm, F), BF16)
        if paired:
            vm["gu_f", s] = ((K, 2, hm, F), F32)
        if once:
            vm["rows_f", s] = ((dp, tp, hr, d), F32)
        for p in ("p1", "p2", "p3"):
            if once and p != "p3":
                vm[p, "_send", s] = ((dp, hr, d), BF16)
                vm[p, "_recv", s] = ((dp, hr, d), BF16)
                vm[p, "_parts", s] = ((R, dp, hr, d), BF16)
            else:
                vm[p, "_send", s] = ((R, hr, d), BF16)
                vm[p, "_recv", s] = ((R - 1, hr, d), BF16)
        vm["f_send", s] = ((K, hm, Wp + LANES), F32)
        vm["f_recv", s] = ((K - 1, hm, Wp + LANES), F32)
        vm["q_send", s] = ((K, 2, hm, Wp), BF16)
        vm["q_recv", s] = ((K - 1, 2, hm, Wp), BF16)
        vm["v_send", s] = ((K, 2, hm, V), BF16)
        vm["v_recv", s] = ((K - 1, 2, hm, V), BF16)
        vm["columns", s] = ((3, W, hm), F32)
        vm["vals", s] = ((hm, V), F32)
        vm["read", s] = ((hm, V), F32)
        vm["hr_all", s] = ((K, hm, V), BF16)
    names = [*ARGS, "result", "new_state", *vm, "local_sem", "send_sem", "recv_sem"]
    chunks = len(SHARES) if paired else CHUNKS
    sems = S * (14 + 2 * (1 + 2 * chunks + max(RELAYED_SUMS)))
    outputs = pl.pallas_call(
        functools.partial(kernel, dims, names),
        out_shape=(
            pltpu.VMEM((mr, d), BF16),
            pltpu.VMEM(ref["st"].shape, F32),
        ),
        in_specs=[pl.BlockSpec(memory_space=pl.ANY)] * len(ARGS),
        out_specs=[pl.BlockSpec(memory_space=pltpu.VMEM)] * 2,
        scratch_shapes=[
            *[pltpu.VMEM(shape, dtype) for shape, dtype in vm.values()],
            pltpu.SemaphoreType.DMA((15 + S + 4 * chunks,)),
            pltpu.SemaphoreType.DMA((sems,)),
            pltpu.SemaphoreType.DMA((sems,)),
        ],
        compiler_params=pltpu.CompilerParams(
            collective_id=0, has_side_effects=True, vmem_limit_bytes=56 * 1024 * 1024
        ),
    )(*[ref[n] for n in ARGS])
    return pl.pallas_call(
        store,
        out_shape=(
            jax.ShapeDtypeStruct((mr, d), BF16),
            jax.ShapeDtypeStruct(ref["st"].shape, F32),
        ),
        in_specs=[pl.BlockSpec(memory_space=pltpu.VMEM)] * 2,
        out_specs=[pl.BlockSpec(memory_space=pl.ANY)] * 2,
        scratch_shapes=[pltpu.SemaphoreType.DMA((2,))],
    )(*[pltpu.with_memory_space_constraint(v, pltpu.VMEM) for v in outputs])


def solution(mesh):
    sizes = (mesh.shape["dp"], mesh.shape["tp"], mesh.shape["kv"])
    return jax.shard_map(
        functools.partial(per_device, sizes),
        mesh=mesh,
        in_specs=(
            P(("grp", "dp", "tp"), "kv"),
            P(("grp", "kv"), ("dp", "tp"), None, None),
            P(("grp", "kv"), ("dp", "tp")),
            P("kv"),
            P("kv", ("dp", "tp")),
            P("kv", ("dp", "tp")),
            P(("dp", "tp"), "kv"),
            P("kv"),
            P("kv", ("dp", "tp")),
            P("kv", ("dp", "tp")),
            P("kv", ("dp", "tp")),
            P("kv", ("dp", "tp")),
            P("kv", ("dp", "tp")),
            P(),
            P(("dp", "tp"), "kv"),
            P("kv"),
            P("kv", ("dp", "tp")),
            P("kv", ("dp", "tp")),
            P(("dp", "tp"), "kv"),
        ),
        out_specs=(P(("grp", "dp", "tp"), "kv"), P(("grp", "kv"), ("dp", "tp"), None, None)),
        check_vma=False,
    )
```

time: 99.3 us -> 75.7 us (0.76)
  Pallas kernels: 93.9 us -> 74.9 us
  local copies, waits for them, and re-layouts: 4.53 us -> 0 us
    pallas_call x1 -> x2, Pallas kernels: 93.9 us -> 74.9 us  [the longest x1 73.6 us: per_device(): pl.pallas_call(functools.partial(kernel, dims, names), out_shape=(pltpu.V...]
    unnamed x2 -> x0, local copies, waits for them, and re-layouts: 4.53 us -> none
where the time goes in v2:
time: 75.7 us; the launch traced here: 75.5 us
  Pallas kernels  74.9 us (99%)
    pallas_call x1, Pallas kernels, per_device(): pl.pallas_call(functools.partial(kernel, dims, names), out_shape=(pltpu.V...  73.6 us

profile of v2, /device:TPU:0, one launch (start us, length us, event | category | flops | bytes accessed | tf_op | source)
XLA Modules:
  0.0 75.5 jit_solution(8928755990363382961)
XLA Ops:
  0.6 73.6 %shard_map.194 = (bf16[16,1024]{1,0:T(8,128)(2,1)S(1)}, f32[16,4,64,128]{3,2,1,0:T(8,128)S(1)}) custom-call(bf16[16,1024]{1,0:T(8,128)(2,1)} %refs_0_.1, f32[16,4,64,128]{3,2,1,0:T(8,128)} %refs_1_.1, f32[16,256]{1,0:T(8,128)} %refs_2_.1, f32[1,1024]{1,0:T(1,128)} %bitcast.4, bf16[1024,2816]{1,0:T(8,128)(2,1)} %refs_4_.1, bf16[1024,2816]{1,0:T(8,128)(2,1)} %refs_5_.1, ...), custom_call_target="tpu_custom_call" | custom-call | tf_op jit(solution)/shard_map/pallas_call | solution.py:638
  74.2 1.3 %shard_map.195 = (bf16[16,1024]{1,0:T(8,128)(2,1)}, f32[16,4,64,128]{3,2,1,0:T(8,128)}) custom-call(bf16[16,1024]{1,0:T(8,128)(2,1)S(1)} %get-tuple-element.4.result, f32[16,4,64,128]{3,2,1,0:T(8,128)S(1)} %get-tuple-element.5.state), custom_call_target="tpu_custom_call" | custom-call | tf_op jit(solution)/shard_map/pallas_call | solution.py:656

commit v3 on v2

--- a/solution.py
+++ b/solution.py
@@ -20,11 +20,11 @@
 RELAYED_SUMS = (3, 3)
 RELAYED_HIDDEN = ((0, 1), ())
 FIRST = (8.9, 9.8, 10.9, 13.0, 14.0, 16.0, 17.0, 19.0, 22.0, 23.0, 25.0, 28.0, 30.0, 32.0)
-FIRST += (33.0, 33.1, 35.0, 38.0, 39.0, 40.0, 41.0, 43.0, 44.0, 44.1, 49.0, 50.0, 52.0, 54.0)
-FIRST += (54.1, 54.2, 55.0, 57.0, 59.0, 62.0, 64.0, 67.0, 69.0, 71.0, 74.0)
-SECOND = (15.0, 18.0, 20.0, 21.0, 24.0, 26.0, 27.0, 33.2, 33.3, 36.0, 36.1, 36.2, 37.0, 37.1)
-SECOND += (42.0, 45.0, 46.0, 47.0, 48.0, 51.0, 53.0, 53.1, 56.0, 58.0, 60.0, 61.0, 63.0, 65.0)
-SECOND += (66.0, 71.1, 71.2, 73.0, 73.1, 73.2, 75.0)
+FIRST += (33.0, 35.0, 38.0, 39.0, 40.0, 41.0, 43.0, 44.0, 49.0, 50.0, 52.0, 54.0, 54.1, 54.2)
+FIRST += (55.0, 57.0, 59.0, 62.0, 64.0, 67.0, 69.0, 71.0, 74.0)
+SECOND = (15.0, 18.0, 20.0, 21.0, 24.0, 26.0, 27.0, 33.2, 33.3, 36.0, 36.1, 36.2, 37.0, 42.0)
+SECOND += (45.0, 46.0, 47.0, 48.0, 51.0, 53.0, 56.0, 58.0, 60.0, 61.0, 63.0, 65.0, 66.0, 71.1)
+SECOND += (71.2, 73.0, 73.1, 73.2, 75.0)
 READY = (FIRST, SECOND)
 
 
@@ -395,8 +395,8 @@
         whole, send, recv, parts = ref["rows_f", s], ref[p, "_send", s], ref[p, "_recv", s], ref[p, "_parts", s]
         whole[...] = value.reshape(DP, TP, hr, d)
         first, second = group(), group()
-        halves = [first[1], arrival()]
-        spans_d = spans(d, 2)
+        halves = [first[1]]
+        spans_d = spans(d, 1)
         for a, b in spans_d:
             send[:, :, a:b] = whole[:, 1 - tp_i, :, a:b].astype(BF16)
             cut = (slice(None), slice(None), pl.ds(a, b - a))

time: 75.7 us -> 75.5 us (level)
  no operation moved by 1% of the time
where the time goes in v3:
time: 75.5 us; the launch traced here: 75.3 us
  Pallas kernels  74.7 us (99%)
    pallas_call x1, Pallas kernels, per_device(): pl.pallas_call(functools.partial(kernel, dims, names), out_shape=(pltpu.V...  73.4 us

profile of v3, /device:TPU:0, one launch (start us, length us, event | category | flops | bytes accessed | tf_op | source)
XLA Modules:
  0.0 75.3 jit_solution(5269190309356793403)
XLA Ops:
  0.6 73.4 %shard_map.194 = (bf16[16,1024]{1,0:T(8,128)(2,1)S(1)}, f32[16,4,64,128]{3,2,1,0:T(8,128)S(1)}) custom-call(bf16[16,1024]{1,0:T(8,128)(2,1)} %refs_0_.1, f32[16,4,64,128]{3,2,1,0:T(8,128)} %refs_1_.1, f32[16,256]{1,0:T(8,128)} %refs_2_.1, f32[1,1024]{1,0:T(1,128)} %bitcast.4, bf16[1024,2816]{1,0:T(8,128)(2,1)} %refs_4_.1, bf16[1024,2816]{1,0:T(8,128)(2,1)} %refs_5_.1, ...), custom_call_target="tpu_custom_call" | custom-call | tf_op jit(solution)/shard_map/pallas_call | solution.py:638
  74.0 1.3 %shard_map.195 = (bf16[16,1024]{1,0:T(8,128)(2,1)}, f32[16,4,64,128]{3,2,1,0:T(8,128)}) custom-call(bf16[16,1024]{1,0:T(8,128)(2,1)S(1)} %get-tuple-element.4.result, f32[16,4,64,128]{3,2,1,0:T(8,128)S(1)} %get-tuple-element.5.state), custom_call_target="tpu_custom_call" | custom-call | tf_op jit(solution)/shard_map/pallas_call | solution.py:656
